TPU v7x, 32 devices: a whole 2x2x4 slice. The times are simulated.
32 devices in a mesh: sp: 8 (over z, y), tp: 4 (over x, core).
Axes of the slice: x: 2, y: 2, z: 4, core: 2. Of those that a mesh axis runs over, the one named last changes fastest.
Arguments:
- queries: bfloat16 [4096, 512], P('sp', 'tp'), may hold values from -6 to 6
- key_matrix: bfloat16 [4096, 512], P('sp', 'tp'), may hold values from -6 to 6
- value_matrix: bfloat16 [4096, 1024], P('sp', 'tp'), may hold values from -6 to 6
- channel_decay_input: bfloat16 [4096, 512], P('sp', 'tp')
- head_decay_offset: float32 [4096, 8], P('sp', 'tp'), may hold values from -1 to 0
- output_gate_input: bfloat16 [4096, 1024], P('sp', 'tp'), may hold values from -6 to 6
- head_norm_gain: float32 [128], replicated, may hold values from 0.1 to 1.9
- residual: bfloat16 [4096, 2048], P(('sp', 'tp')), may hold values from -6 to 6
- mixer_output_weight: bfloat16 [1024, 2048], replicated, may hold values from -0.1875 to 0.1875
- expert_norm_gain: float32 [2048], replicated, may hold values from 0.1 to 1.9
- routes: int32 [4096, 4], P(('sp', 'tp')), may hold values from 0 to 63, all different within a row; in each aligned block of 128 rows (0 to 127, 128 to 255, ...) at most 16 rows name the same one
- chosen_router_scores: float32 [4096, 4], P(('sp', 'tp')), may hold values from 0.1 to 1
- routed_gate_weight: bfloat16 [64, 2048, 512], P(('sp', 'tp')), may hold values from -0.125 to 0.125
- routed_up_weight: bfloat16 [64, 2048, 512], P(('sp', 'tp')), may hold values from -0.125 to 0.125
- routed_down_weight: bfloat16 [64, 512, 2048], P(('sp', 'tp')), may hold values from -0.25 to 0.25
- common_gate_weight: bfloat16 [2048, 512], replicated, may hold values from -0.125 to 0.125
- common_up_weight: bfloat16 [2048, 512], replicated, may hold values from -0.125 to 0.125
- common_down_weight: bfloat16 [512, 2048], replicated, may hold values from -0.25 to 0.25
Outputs:
- layer_out: bfloat16 [4096, 2048], P(('sp', 'tp'))
Inputs may be any that keep to these rules, and one draw needn't show every extreme that they name: `routes`: each row names 4 different experts. In each aligned block of 128 rows (the rows of one device) no expert is named by more than 16 rows, a bound that some block reaches.
All inputs are finite; a program needn't handle non-finite values.
Results may differ from a plain program's by a relative error of at most 0.017.
Values may be sent and summed in bfloat16 or wider, within the bound.
A program may use at most 128 MiB of HBM per device.

v0:
```python
import jax
import jax.numpy as jnp
from jax import lax
from jax.sharding import PartitionSpec as P

D = 2048
KEY_CHANNELS = 64
VDIM = 128
BLOCK = 64
TOP_K = 4


eps_norm = 1e-06
decay_running = 16.0
routed_scale = 2.5


def carried_in(part, axis, combine, identity):
    place = lax.axis_index(axis)
    gathered = jax.tree.map(lambda a: lax.all_gather(a, axis), part)
    state = jax.tree.map(lambda a, e: jnp.zeros_like(a) + jnp.asarray(e, a.dtype), part, identity)

    def one(hop, state):
        return combine(
            state, jax.tree.map(lambda a: lax.dynamic_index_in_dim(a, hop, 0, False), gathered)
        )

    return lax.fori_loop(0, place, one, state)


def expert_block(picked_rows, gate_weight, up_weight, down_weight):
    gate_pre = jnp.dot(picked_rows, gate_weight, preferred_element_type=jnp.float32)
    up_pre = jnp.dot(picked_rows, up_weight, preferred_element_type=jnp.float32)
    hidden = (jax.nn.silu(gate_pre) * up_pre).astype(jnp.bfloat16)
    return jnp.dot(hidden, down_weight, preferred_element_type=jnp.float32)


def apply_experts(arrived, routed_gate_weight, routed_up_weight, routed_down_weight):
    gate_pre = jnp.einsum(
        "sech,ehf->secf", arrived, routed_gate_weight, preferred_element_type=jnp.float32
    )
    up_pre = jnp.einsum(
        "sech,ehf->secf", arrived, routed_up_weight, preferred_element_type=jnp.float32
    )
    hidden = (jax.nn.silu(gate_pre) * up_pre).astype(jnp.bfloat16)
    return jnp.einsum(
        "secf,efh->sech", hidden, routed_down_weight, preferred_element_type=jnp.float32
    ).astype(jnp.bfloat16)


def chain_join(earlier, latter):
    return (earlier[0] * latter[0], latter[0][..., None] * earlier[1] + latter[1])


def on_device(
    queries,
    key_matrix,
    value_matrix,
    channel_decay_input,
    head_decay_offset,
    output_gate_input,
    head_norm_gain,
    residual,
    mixer_output_weight,
    expert_norm_gain,
    routes,
    chosen_router_scores,
    routed_gate_weight,
    routed_up_weight,
    routed_down_weight,
    common_gate_weight,
    common_up_weight,
    common_down_weight,
):
    device_heads = head_decay_offset.shape[1]
    seq_rows = queries.shape[0]
    blocks = seq_rows // BLOCK

    def split_local(values, columns):
        return (
            values.astype(jnp.float32)
            .reshape(blocks, BLOCK, device_heads, columns)
            .transpose(2, 0, 1, 3)
        )

    decay_spike_columns = jnp.repeat(head_decay_offset, KEY_CHANNELS, axis=1)
    decay_logarithm = (
        jax.nn.log_sigmoid(channel_decay_input.astype(jnp.float32)) / decay_running
        + decay_spike_columns
    )
    within = jnp.cumsum(split_local(decay_logarithm, KEY_CHANNELS), axis=2)
    block_end = within[:, :, -1, :]
    q_heads = split_local(queries, KEY_CHANNELS) * KEY_CHANNELS ** (-0.5)
    k_heads = split_local(key_matrix, KEY_CHANNELS)
    v_heads = split_local(value_matrix, VDIM)
    q_decay = q_heads * jnp.exp(within)
    k_grow = k_heads * jnp.exp(-within)
    k_tail = k_heads * jnp.exp(block_end[:, :, None, :] - within)
    causal = jnp.tril(jnp.ones((BLOCK, BLOCK), dtype=bool))
    scores = jnp.where(causal, jnp.einsum("hnid,hnjd->hnij", q_decay, k_grow), 0.0)
    inside = jnp.einsum("hnij,hnje->hnie", scores, v_heads)
    block_state = jnp.einsum("hncd,hnce->hnde", k_tail, v_heads)
    inclusive = jnp.cumsum(block_end, axis=1)
    exclusive = inclusive - block_end
    before = jnp.arange(blocks)[:, None] > jnp.arange(blocks)[None, :]
    spread = jnp.exp(
        jnp.where(
            before[None, :, :, None], exclusive[:, :, None, :] - inclusive[:, None, :, :], -jnp.inf
        )
    )
    local_start = jnp.einsum("hnmd,hmde->hnde", spread, block_state)
    total_log = inclusive[:, -1, :]
    tail_weight = jnp.exp(total_log[:, None, :] - inclusive)
    device_state = jnp.einsum("hnd,hnde->hde", tail_weight, block_state)
    device_decay = jnp.exp(total_log)
    identity = (jnp.ones_like(device_decay), jnp.zeros_like(device_state))
    _, carried = carried_in((device_decay, device_state), "sp", chain_join, identity)
    entering = local_start + jnp.exp(exclusive)[..., None] * carried[:, None, :, :]
    output = inside + jnp.einsum("hncd,hnde->hnce", q_decay, entering)
    output = output.transpose(1, 2, 0, 3).reshape(seq_rows, device_heads, VDIM)
    inv_rms = lax.rsqrt(jnp.mean(output * output, axis=-1, keepdims=True) + eps_norm)
    normed_heads = (output * inv_rms * head_norm_gain).reshape(seq_rows, device_heads * VDIM)
    gated_output = (normed_heads * jax.nn.silu(output_gate_input.astype(jnp.float32))).astype(
        jnp.bfloat16
    )
    tok_count = residual.shape[0]
    stacked = gated_output.reshape(lax.axis_size("tp"), tok_count, gated_output.shape[1])
    projected = jnp.dot(
        lax.all_to_all(stacked, "tp", split_axis=0, concat_axis=2, tiled=True)[0],
        mixer_output_weight,
        preferred_element_type=jnp.float32,
    )[None][0]
    middle = (residual.astype(jnp.float32) + projected).astype(jnp.bfloat16)
    middle_wide = middle.astype(jnp.float32)
    norm_scale = lax.rsqrt(jnp.mean(middle_wide * middle_wide, axis=-1, keepdims=True) + eps_norm)
    normed = (middle_wide * norm_scale * expert_norm_gain).astype(jnp.bfloat16)
    weights = (
        routed_scale * chosen_router_scores / jnp.sum(chosen_router_scores, axis=-1, keepdims=True)
    )
    devices = lax.axis_size("sp") * lax.axis_size("tp")
    exp_dev = routed_gate_weight.shape[0]
    experts_all = exp_dev * devices
    cap_slots = 2 * TOP_K * tok_count // experts_all
    flat_expert = routes.reshape(-1)
    one_hot = (flat_expert[:, None] == jnp.arange(experts_all, dtype=jnp.int32)[None, :]).astype(
        jnp.int32
    )
    slot_index = jnp.sum((jnp.cumsum(one_hot, axis=0) - 1) * one_hot, axis=1)
    destination = flat_expert * cap_slots + slot_index
    buffer_rows = experts_all * cap_slots
    row_owner = jnp.arange(flat_expert.shape[0], dtype=jnp.int32) // TOP_K
    source_row = jnp.full((buffer_rows,), tok_count, jnp.int32).at[destination].set(row_owner)
    normed_pad = jnp.concatenate([normed, jnp.zeros((1, D), jnp.bfloat16)], axis=0)
    outgoing = normed_pad[source_row].reshape(devices, exp_dev, cap_slots, D)
    produced = apply_experts(
        lax.all_to_all(outgoing, ("sp", "tp"), split_axis=0, concat_axis=0, tiled=True),
        routed_gate_weight,
        routed_up_weight,
        routed_down_weight,
    )
    returned = lax.all_to_all(produced, ("sp", "tp"), split_axis=0, concat_axis=0, tiled=True)
    flat_back = returned.reshape(buffer_rows, D)
    gathered = flat_back[destination].reshape(tok_count, TOP_K, D)
    routed = jnp.sum(weights[:, :, None] * gathered, axis=1)
    shared = expert_block(normed, common_gate_weight, common_up_weight, common_down_weight)
    return (middle_wide + routed + shared).astype(jnp.bfloat16)


def solution(mesh):
    placed = (
        P("sp", "tp"),
        P("sp", "tp"),
        P("sp", "tp"),
        P("sp", "tp"),
        P("sp", "tp"),
        P("sp", "tp"),
        P(),
        P(("sp", "tp"), None),
        P(),
        P(),
        P(("sp", "tp"), None),
        P(("sp", "tp"), None),
        P(("sp", "tp"), None, None),
        P(("sp", "tp"), None, None),
        P(("sp", "tp"), None, None),
        P(),
        P(),
        P(),
    )
    return jax.shard_map(
        on_device, mesh=mesh, in_specs=placed, out_specs=P(("sp", "tp"), None), check_vma=False
    )
```

profile of v0, /device:TPU:0, one launch (start us, length us, event | category | flops | bytes accessed | tf_op | source)
XLA Modules:
  0.0 336.8 jit_solution(10941217069375739230)
XLA Ops:
  9.7 2.0 reshape.194
  11.8 2.0 bitcast_multiply_fusion.3
  14.7 33.0 %all-gather.1 = f32[16,64,128]{2,1,0:T(8,128)S(1)} all-gather(f32[2,64,128]{2,1,0:T(8,128)S(1)} %bitcast.150), channel_id=3, replica_groups=mesh['sp'=8,'tp'=4] {'sp'}, dimensions={0}, use_global_device_ids=true | all-gather | bytes 589824 | tf_op jit(solution)/shard_map/all_gather | solution.py:20
  47.8 20.7 %all-gather = f32[16,1,64]{2,1,0:T(1,128)S(1)} all-gather(f32[2,1,64]{2,1,0:T(1,128)S(1)} %copy-done.12), channel_id=2, replica_groups=mesh['sp'=8,'tp'=4] {'sp'}, dimensions={0}, use_global_device_ids=true | all-gather | bytes 4608 | tf_op jit(solution)/shard_map/all_gather | solution.py:20
  68.5 1.4 copy.53
  69.9 1.4 copy.56
  71.7 1.5 fusion.27
  74.4 1.5 copy.59
  77.5 3.4 %all-to-all-start = ((bf16[4,128,256]{1,2,0:T(8,128)(2,1)}), bf16[4,128,256]{1,2,0:T(8,128)(2,1)S(1)}, u32[]{:S(2)}, u32[]{:S(2)}) async-start(bf16[4,128,256]{1,2,0:T(8,128)(2,1)} %copy.61), calls=%async_computation | async-start | bytes 524288 | tf_op jit(solution)/shard_map/all_to_all | solution.py:129
  83.1 2.4 scatter_custom_fusion
  86.9 3.1 multiply_reduce_fusion.1
  91.2 6.0 %gather_fusion = bf16[1024,2048]{1,0:T(8,128)(2,1)} fusion(bf16[129,2048]{1,0:T(8,128)(2,1)S(1)} %concatenate.3, s32[1024]{0:T(1024)S(1)} %fusion.75), kind=kCustom, calls=%fused_computation | custom fusion | bytes 8392704 | tf_op jit(solution)/shard_map/gather | solution.py:154
  97.2 96.9 %all_to_all.25 = bf16[32,2,16,2048]{3,2,1,0:T(8,128)(2,1)S(1)} all-to-all(bf16[32,2,16,2048]{3,2,1,0:T(8,128)(2,1)} %bitcast.143), channel_id=1, replica_groups=mesh['sp'=8,'tp'=4] {'sp','tp'}, dimensions={0} | all-to-all | bytes 8388608 | tf_op jit(solution)/shard_map/all_to_all | solution.py:156
  194.1 2.0 copy-done.4
  196.1 3.7 %fusion.4 = f32[2,32,16,512]{3,2,1,0:T(8,128)} fusion(bf16[2,2048,512]{2,1,0:T(8,128)(2,1)S(1)} %copy-done.13, bf16[32,2,16,2048]{3,2,1,0:T(8,128)(2,1)S(1)} %all_to_all.25), kind=kOutput, calls=%fused_computation.9 | convolution fusion | flops 2147483648 | bytes 10485760 | tf_op jit(solution)/shard_map/sech,ehf->secf/dot_general | solution.py:39
  199.8 11.8 %convert_bitcast_fusion = bf16[32,2,16,2048]{3,2,0,1:T(8,128)(2,1)} fusion(bf16[2,512,2048]{2,1,0:T(8,128)(2,1)} %param.34, f32[2,32,16,512]{3,2,1,0:T(8,128)} %fusion.4, bf16[2,2048,512]{2,1,0:T(8,128)(2,1)} %param.33, bf16[32,2,16,2048]{3,2,1,0:T(8,128)(2,1)} %copy-done.4), kind=kOutput, calls=%fused_computation.12 | convolution fusion | flops 4300210176 | bytes 18874368 | tf_op jit(solution)/shard_map/secf,efh->sech/dot_general | solution.py:46
  211.6 4.7 %copy.69 = bf16[32,2,16,2048]{3,2,1,0:T(8,128)(2,1)} copy(bf16[32,2,16,2048]{3,2,0,1:T(8,128)(2,1)} %convert_bitcast_fusion) | data formatting | bytes 8388608 | tf_op jit(solution)/shard_map/convert_element_type | solution.py:48
  216.3 3.9 %all-to-all-start.2 = ((bf16[32,2,16,2048]{3,2,1,0:T(8,128)(2,1)}), bf16[32,2,16,2048]{3,2,1,0:T(8,128)(2,1)}, u32[]{:S(2)}, u32[]{:S(2)}) async-start(bf16[32,2,16,2048]{3,2,1,0:T(8,128)(2,1)} %copy.69), calls=%async_computation.2 | async-start | bytes 8388608 | tf_op jit(solution)/shard_map/all_to_all | solution.py:161
  220.5 2.0 fusion.86
  222.5 91.5 %all-to-all-done.2 = bf16[32,2,16,2048]{3,2,1,0:T(8,128)(2,1)} async-done(((bf16[32,2,16,2048]{3,2,1,0:T(8,128)(2,1)}), bf16[32,2,16,2048]{3,2,1,0:T(8,128)(2,1)}, u32[]{:S(2)}, u32[]{:S(2)}) %all-to-all-start.2) | async-done | bytes 4194336 | tf_op jit(solution)/shard_map/all_to_all | solution.py:161
  314.0 8.0 %gather_fusion.1 = bf16[512,2048]{1,0:T(8,128)(2,1)} fusion(bf16[1024,2048]{1,0:T(8,128)(2,1)} %bitcast.37, s32[1024]{0:T(1024)S(1)} %pad_clamp_fusion), kind=kCustom, calls=%fused_computation.1 | custom fusion | bytes 4196352 | tf_op jit(solution)/shard_map/gather | solution.py:163
  322.0 4.8 %reshape.159 = f32[128,4,2048]{2,1,0:T(4,128)} reshape(bf16[512,2048]{1,0:T(8,128)(2,1)} %gather_fusion.1) | data formatting | bytes 6291456 | tf_op jit(solution)/shard_map/convert_element_type | solution.py:164
  326.7 6.4 %multiply_reduce_fusion = f32[128,2048]{1,0:T(8,128)} fusion(f32[128,4,2048]{2,1,0:T(4,128)} %reshape.159, f32[128,4]{1,0:T(8,128)S(1)} %copy.62), kind=kLoop, calls=%fused_computation.11 | loop fusion | flops 1835008 | bytes 5244928 | tf_op jit(solution)/shard_map/reduce_sum | solution.py:164
  333.1 3.7 %fusion.12 = bf16[128,2048]{1,0:T(8,128)(2,1)} fusion(bf16[512,2048]{1,0:T(8,128)(2,1)S(1)} %copy-done, bf16[128,2048]{1,0:T(8,128)(2,1)} %copy-done.3, bf16[2048,512]{1,0:T(8,128)(2,1)} %param.36, f32[128,2048]{1,0:T(8,128)S(1)} %copy-done.2, f32[128,2048]{1,0:T(8,128)} %multiply_reduce_fusion, f32[128,512]{1,0:T(8,128)S(1)} %fusion.86), kind=kOutput, calls=%fused_computation.19 | convolution fusion | flops 538050560 | bytes 7602176 | tf_op jit(solution)/shard_map/dot_general | solution.py:35
  (82 shorter events, 18.7 us)
Async XLA Ops:
  0.0 333.1 %copy-start = (bf16[512,2048]{1,0:T(8,128)(2,1)S(1)}, bf16[512,2048]{1,0:T(8,128)(2,1)}, u32[]{:S(2)}) copy-start(bf16[512,2048]{1,0:T(8,128)(2,1)} %param.37) | copy-start | bytes 6291460
  0.0 11.7 %copy-start.6 = (bf16[512,256]{1,0:T(8,128)(2,1)S(1)}, bf16[512,256]{1,0:T(8,128)(2,1)}, u32[]{:S(2)}) copy-start(bf16[512,256]{1,0:T(8,128)(2,1)} %param.22) | copy-start | bytes 786436
  9.7 4.4 %copy-start.8 = (bf16[2,8,64,1]{1,3,2,0:T(2,128)(2,1)S(1)}, bf16[2,8,64,1]{1,3,2,0:T(2,128)(2,1)}, u32[]{:S(2)}) copy-start(bf16[2,8,64,1]{1,3,2,0:T(2,128)(2,1)} %copy.70) | copy-start | bytes 6148
  11.8 36.0 %copy-start.12 = (f32[2,1,64]{2,1,0:T(1,128)S(1)}, f32[2,1,64]{2,1,0:T(1,128)}, u32[]{:S(2)}) copy-start(f32[2,1,64]{2,1,0:T(1,128)} %get-tuple-element.64) | copy-start | bytes 1540
  14.0 0.7 copy-start.5
  68.5 7.4 %copy-start.14 = (f32[128]{0:T(128)S(1)}, f32[128]{0:T(128)}, u32[]{:S(2)}) copy-start(f32[128]{0:T(128)} %param.26) | copy-start | bytes 1540
  71.7 4.8 %copy-start.7 = (bf16[512,256]{1,0:T(8,128)(2,1)S(1)}, bf16[512,256]{1,0:T(8,128)(2,1)}, u32[]{:S(2)}) copy-start(bf16[512,256]{1,0:T(8,128)(2,1)} %param.25) | copy-start | bytes 786436
  71.7 9.2 %copy-start.10 = (s32[128,4]{0,1:T(4,128)S(1)}, s32[128,4]{0,1:T(4,128)}, u32[]{:S(2)}) copy-start(s32[128,4]{0,1:T(4,128)} %param.30) | copy-start | bytes 6148
  76.6 14.3 %copy-start.9 = (f32[2048]{0:T(1024)S(1)}, f32[2048]{0:T(1024)}, u32[]{:S(2)}) copy-start(f32[2048]{0:T(1024)} %param.29) | copy-start | bytes 24580
  77.5 9.4 %all-to-all-start = ((bf16[4,128,256]{1,2,0:T(8,128)(2,1)}), bf16[4,128,256]{1,2,0:T(8,128)(2,1)S(1)}, u32[]{:S(2)}, u32[]{:S(2)}) async-start(bf16[4,128,256]{1,2,0:T(8,128)(2,1)} %copy.61), calls=%async_computation | async-start | bytes 524288 | tf_op jit(solution)/shard_map/all_to_all | solution.py:129
  90.0 1.0 copy-start.1
  91.1 129.3 %copy-start.3 = (bf16[128,2048]{1,0:T(8,128)(2,1)}, bf16[128,2048]{1,0:T(8,128)(2,1)S(1)}, u32[]{:S(2)}) copy-start(bf16[128,2048]{1,0:T(8,128)(2,1)S(1)} %multiply_convert_fusion) | copy-start | bytes 1572868
  97.2 98.9 %copy-start.13 = (bf16[2,2048,512]{2,1,0:T(8,128)(2,1)S(1)}, bf16[2,2048,512]{2,1,0:T(8,128)(2,1)}, u32[]{:S(2)}) copy-start(bf16[2,2048,512]{2,1,0:T(8,128)(2,1)} %param.32) | copy-start | bytes 12582916
  194.1 2.0 copy-start.4
  216.3 4.0 %copy-start.11 = (f32[128,4]{0,1:T(4,128)S(1)}, f32[128,4]{0,1:T(4,128)}, u32[]{:S(2)}) copy-start(f32[128,4]{0,1:T(4,128)} %param.31) | copy-start | bytes 6148
  216.3 97.6 %all-to-all-start.2 = ((bf16[32,2,16,2048]{3,2,1,0:T(8,128)(2,1)}), bf16[32,2,16,2048]{3,2,1,0:T(8,128)(2,1)}, u32[]{:S(2)}, u32[]{:S(2)}) async-start(bf16[32,2,16,2048]{3,2,1,0:T(8,128)(2,1)} %copy.69), calls=%async_computation.2 | async-start | bytes 8388608 | tf_op jit(solution)/shard_map/all_to_all | solution.py:161
  326.7 6.4 %copy-start.2 = (f32[128,2048]{1,0:T(8,128)S(1)}, f32[128,2048]{1,0:T(8,128)}, u32[]{:S(2)}) copy-start(f32[128,2048]{1,0:T(8,128)} %copy-done.1) | copy-start | bytes 3145732
where the time goes:
time: 338 us; the launch traced here: 337 us
  blocking collectives  151 us (45%)
  waiting for transfers between devices  92.8 us (27%)
  local copies, waits for them, and re-layouts  43.2 us (13%)
  matrix products  27.7 us (8%)
  other arithmetic  14.9 us (4%)
  starting transfers between devices  7.35 us (2%)
    all_to_all x1, blocking collectives, on_device(): lax.all_to_all(outgoing, ('sp', 'tp'), split_axis=0, concat_axis=0, tiled...  96.9 us
    all_to_all x1, waiting for transfers between devices, on_device(): lax.all_to_all(produced, ('sp', 'tp'), split_axis=0, concat_axis=0, tiled...  91.5 us
    all_gather x2, blocking collectives, carried_in(): gathered = jax.tree.map(lambda a: lax.all_gather(a, axis), part)  53.7 us
    dot_general x1, matrix products, apply_experts(): jnp.einsum('secf,efh->sech', hidden, routed_down_weight, preferred_elemen...  11.8 us
    gather x1, local copies, waits for them, and re-layouts, on_device(): gathered = flat_back[destination].reshape(tok_count, TOP_K, D)  8 us
  transfers between devices with their start and end apart: 2, of which 2 were waited for; matrix products, arithmetic and copies ran while one was open for 2% of the time, Pallas kernels for 0%

commit v1 on v0

v1 whole, which is shorter than its diff:
```python
import functools
import math

import jax
import jax.numpy as jnp
from jax import lax
from jax.experimental import pallas as pl
from jax.experimental.pallas import tpu as pltpu
from jax.sharding import PartitionSpec as P

D = 2048
KEY_CHANNELS = 64
VDIM = 128
BLOCK = 64
TOP_K = 4


eps_norm = 1e-06
decay_running = 16.0
routed_scale = 2.5


def peer(sp, tp):
    return {"sp": sp, "tp": tp}


def greet(targets):
    barrier = pltpu.get_barrier_semaphore()
    for target in targets:
        pl.semaphore_signal(
            barrier, inc=1, device_id=target, device_id_type=pl.DeviceIdType.MESH
        )
    pl.semaphore_wait(barrier, len(targets))


def remote(src, dst, send, recv, target):
    return pltpu.make_async_remote_copy(
        src_ref=src,
        dst_ref=dst,
        send_sem=send,
        recv_sem=recv,
        device_id=target,
        device_id_type=pl.DeviceIdType.MESH,
    )


def remote_call(kernel, out_shape, operands, scratch, number, flops=1_000_000):
    multi = isinstance(out_shape, (tuple, list))
    vmem = pl.BlockSpec(memory_space=pltpu.VMEM)
    return pl.pallas_call(
        kernel,
        out_shape=out_shape,
        in_specs=[vmem] * len(operands),
        out_specs=[vmem] * len(out_shape) if multi else vmem,
        scratch_shapes=scratch,
        compiler_params=pltpu.CompilerParams(
            collective_id=number, has_side_effects=True, vmem_limit_bytes=56 * 1024 * 1024
        ),
    )(*operands)


def gather_sp_kernel(count, x_ref, y_ref, xs_ref, ys_ref, send, recv):
    me, tp = lax.axis_index("sp"), lax.axis_index("tp")
    targets = [peer(lax.rem(me + d, count), tp) for d in range(1, count)]
    greet(targets)
    copies = []
    for d in range(1, count):
        for i, (src, dst) in enumerate(((x_ref, xs_ref), (y_ref, ys_ref))):
            copies.append(
                remote(src, dst.at[me], send.at[i, d], recv.at[i, d], targets[d - 1])
            )
            copies[-1].start()
    xs_ref[me] = x_ref[...]
    ys_ref[me] = y_ref[...]
    for copy in copies:
        copy.wait()


def gather_sp(state, packet):
    count = lax.axis_size("sp")
    return remote_call(
        functools.partial(gather_sp_kernel, count),
        [
            jax.ShapeDtypeStruct((count,) + state.shape, state.dtype),
            jax.ShapeDtypeStruct((count,) + packet.shape, packet.dtype),
        ],
        [state, packet],
        [pltpu.SemaphoreType.DMA((2, count)), pltpu.SemaphoreType.DMA((2, count))],
        0,
    )


def swap_tp_kernel(count, x_ref, out_ref, send, recv):
    sp, me = lax.axis_index("sp"), lax.axis_index("tp")
    width = x_ref.shape[2]
    targets = [peer(sp, lax.rem(me + d, count)) for d in range(1, count)]
    greet(targets)
    columns = pl.ds(pl.multiple_of(me * width, width), width)
    copies = []
    for d in range(1, count):
        copies.append(
            remote(
                x_ref.at[lax.rem(me + d, count)],
                out_ref.at[:, columns],
                send.at[d],
                recv.at[d],
                targets[d - 1],
            )
        )
        copies[-1].start()
    out_ref[:, columns] = x_ref[me]
    for copy in copies:
        copy.wait()


def swap_tp(stacked):
    count = lax.axis_size("tp")
    return remote_call(
        functools.partial(swap_tp_kernel, count),
        jax.ShapeDtypeStruct((stacked.shape[1], count * stacked.shape[2]), stacked.dtype),
        [stacked],
        [pltpu.SemaphoreType.DMA((count,)), pltpu.SemaphoreType.DMA((count,))],
        1,
    )


class Place:
    def __init__(self, sp_size, tp_size):
        self.deep = math.gcd(sp_size, 4)
        self.rows = sp_size // self.deep
        self.tp_size = tp_size
        self.flat = self.rows * tp_size

    def here(self):
        sp, tp = lax.axis_index("sp"), lax.axis_index("tp")
        self.sp, self.tp = sp, tp
        self.a = sp // self.rows
        self.b = lax.rem(sp, self.rows)
        self.p = self.b * self.tp_size + tp
        return self

    def column(self, a):
        return peer(a * self.rows + self.b, self.tp)

    def plane(self, p):
        return peer(self.a * self.rows + p // self.tp_size, lax.rem(p, self.tp_size))

    def across(self, q):
        return lax.rem(self.p + q, self.flat)

    def nearest(self, i):
        last = self.deep - 1
        span = jnp.minimum(self.a, last - self.a)
        zigzag = self.a + ((i + 1) // 2 if i % 2 else -(i // 2))
        return jnp.where(i <= 2 * span, zigzag, jnp.where(self.a < last - self.a, i, last - i))


def tiles_of(width, most=512):
    step = math.gcd(width, most)
    return [slice(i, i + step) for i in range(0, width, step)]


def flatten_rows(block):
    groups, rows, width = block.shape
    if rows % 16 == 0:
        return block.reshape(groups * rows, width)
    return block.astype(jnp.float32).reshape(groups * rows, width).astype(jnp.bfloat16)


def experts_kernel(
    sizes, x_ref, middle_ref, select_ref, mix_ref, gate_ref, up_ref, down_ref,
    wide_gate, wide_up, wide_down, out_ref,
    column_ref, stage_ref, arrived_ref, made_ref, back_ref, sent_ref, came_ref, base_ref,
    hidden_ref, own_gate, own_up, own_down,
    weight_sem, zs, zr, ps, pr, bs, br, ss, sr,
):
    at = Place(*sizes).here()
    last = at.deep - 1
    flat, rows = stage_ref.shape[1], stage_ref.shape[2]
    width = x_ref.shape[1]
    experts = own_gate.shape[0]
    cap = rows // experts
    loads = [
        pltpu.make_async_copy(wide_gate, own_gate, weight_sem.at[0]),
        pltpu.make_async_copy(wide_up, own_up, weight_sem.at[1]),
        pltpu.make_async_copy(wide_down, own_down, weight_sem.at[2]),
    ]
    for load in loads:
        load.start()
    has_right, has_left = at.a < last, at.a > 0
    greet(
        [at.column(lax.rem(at.a + d, at.deep)) for d in range(1, at.deep)]
        + [at.plane(at.across(q)) for q in range(1, flat)]
    )

    def relay(source, owner, side):
        return remote(
            source,
            column_ref.at[owner],
            zs.at[side, owner],
            zr.at[owner],
            at.column(at.a + (1 if side == 0 else -1)),
        )

    def sends(owner):
        right = has_right & (owner <= at.a)
        left = has_left & (owner >= at.a)
        return right, left

    def forward(source, owner):
        right, left = sends(owner)
        pl.when(right)(lambda: relay(source, owner, 0).start())
        pl.when(left)(lambda: relay(source, owner, 1).start())

    def out_copy(owner, q):
        target = at.across(q)
        return remote(
            stage_ref.at[owner, target],
            arrived_ref.at[owner, at.p],
            ps.at[owner, q],
            pr.at[owner, q],
            at.plane(target),
        )

    def back_copy(owner, q):
        target = at.across(q)
        return remote(
            made_ref.at[owner, target],
            back_ref.at[owner, at.p],
            bs.at[owner, q],
            br.at[owner, q],
            at.plane(target),
        )

    def pass_on(owner, source):
        for cut in tiles_of(width):
            picked = jnp.dot(
                select_ref[owner], source[:, cut], preferred_element_type=jnp.float32
            )
            stage_ref[owner, :, :, cut] = picked.reshape(flat, rows, -1).astype(jnp.bfloat16)
        for q in range(1, flat):
            out_copy(owner, q).start()
        arrived_ref[owner, at.p] = stage_ref[owner, at.p]

    def run_experts(owner):
        for q in range(1, flat):
            out_copy(owner, q).wait_recv()
        for e in range(experts):
            mine = slice(e * cap, (e + 1) * cap)
            for cut in tiles_of(own_gate.shape[2], 256):
                block = flatten_rows(arrived_ref[owner, :, mine, :])
                gate = jnp.dot(block, own_gate[e, :, cut], preferred_element_type=jnp.float32)
                up = jnp.dot(block, own_up[e, :, cut], preferred_element_type=jnp.float32)
                hidden_ref[:, cut] = (jax.nn.silu(gate) * up).astype(jnp.bfloat16)
            for cut in tiles_of(width):
                down = jnp.dot(
                    hidden_ref[...], own_down[e, :, cut], preferred_element_type=jnp.float32
                )
                made_ref[owner, :, mine, cut] = down.reshape(flat, cap, -1).astype(jnp.bfloat16)
        for q in range(1, flat):
            back_copy(owner, q).start()
        back_ref[owner, at.p] = made_ref[owner, at.p]

    order = [at.nearest(i) for i in range(at.deep)]
    forward(x_ref, at.a)
    pass_on(at.a, x_ref)
    tokens = x_ref.shape[0]
    for cut in tiles_of(gate_ref.shape[1], 256):
        gate = jnp.dot(x_ref[...], gate_ref[:, cut], preferred_element_type=jnp.float32)
        up = jnp.dot(x_ref[...], up_ref[:, cut], preferred_element_type=jnp.float32)
        sent_ref[at.a, :, cut] = (jax.nn.silu(gate) * up).astype(jnp.bfloat16)
    for cut in tiles_of(width):
        base_ref[:, cut] = middle_ref[:, cut].astype(jnp.float32) + jnp.dot(
            sent_ref[at.a, :, : gate_ref.shape[1]],
            down_ref[:, cut],
            preferred_element_type=jnp.float32,
        )
    for i in range(1, at.deep + 1):
        if i < at.deep:
            relay(x_ref, order[i], 0).wait_recv()
            forward(column_ref.at[order[i]], order[i])
            pass_on(order[i], column_ref.at[order[i]])
        if i == 1:
            for load in loads:
                load.wait()
        run_experts(order[i - 1])

    def gather_back(owner):
        for q in range(1, flat):
            back_copy(owner, q).wait_recv()

    def mixed(owner, cut):
        block = flatten_rows(back_ref[owner, :, :, cut])
        return jnp.dot(mix_ref[owner], block, preferred_element_type=jnp.float32)

    def toward(owner, side):
        return remote(
            sent_ref.at[owner],
            came_ref.at[side, owner],
            ss.at[owner],
            sr.at[side, owner],
            at.column(at.a + (-1 if side == 0 else 1)),
        )

    def step(owner, side, more):
        for cut in tiles_of(width):
            part = mixed(owner, cut)
            if more:
                part = part + came_ref[side, owner, :, cut].astype(jnp.float32)
            sent_ref[owner, :, cut] = part.astype(jnp.bfloat16)
        toward(owner, side).start()

    for i in range(at.deep - 1, 0, -1):
        owner = order[i]
        gather_back(owner)
        for side, goes, far in ((0, owner < at.a, has_right), (1, owner > at.a, has_left)):

            @pl.when(goes & far)
            def _(owner=owner, side=side):
                toward(owner, side).wait_recv()
                step(owner, side, True)

            @pl.when(goes & jnp.logical_not(far))
            def _(owner=owner, side=side):
                step(owner, side, False)

    gather_back(at.a)
    for cut in tiles_of(width):
        base_ref[:, cut] += mixed(at.a, cut)
    for side, far in ((0, has_right), (1, has_left)):

        @pl.when(far)
        def _(side=side):
            toward(at.a, side).wait_recv()
            for cut in tiles_of(width):
                base_ref[:, cut] += came_ref[side, at.a, :, cut].astype(jnp.float32)

    out_ref[...] = base_ref[...].astype(out_ref.dtype)
    for i in range(at.deep):
        owner = order[i]
        right, left = sends(owner)
        pl.when(right)(lambda owner=owner: relay(x_ref, owner, 0).wait_send())
        pl.when(left)(lambda owner=owner: relay(x_ref, owner, 1).wait_send())
        for q in range(1, flat):
            out_copy(owner, q).wait_send()
            back_copy(owner, q).wait_send()
        if i > 0:
            toward(owner, 0).wait_send()


def experts_layer(normed, middle, select, mix, common, routed):
    sizes = (lax.axis_size("sp"), lax.axis_size("tp"))
    at = Place(*sizes)
    tokens, width = normed.shape
    slots = select.shape[1]
    box = (at.deep, at.flat, slots // at.flat, width)
    chunk = (at.deep, tokens, width)
    dma = pltpu.SemaphoreType.DMA
    half = jnp.bfloat16
    vmem = pl.BlockSpec(memory_space=pltpu.VMEM)
    far = pl.BlockSpec(memory_space=pl.ANY)
    experts = routed[0].shape[0]
    return pl.pallas_call(
        functools.partial(experts_kernel, sizes),
        out_shape=jax.ShapeDtypeStruct((tokens, width), half),
        in_specs=[vmem] * 7 + [far] * 3,
        out_specs=vmem,
        scratch_shapes=[
            pltpu.VMEM(chunk, half),
            pltpu.VMEM(box, half),
            pltpu.VMEM(box, half),
            pltpu.VMEM(box, half),
            pltpu.VMEM(box, half),
            pltpu.VMEM(chunk, half),
            pltpu.VMEM((2,) + chunk, half),
            pltpu.VMEM((tokens, width), jnp.float32),
            pltpu.VMEM((slots // experts, routed[0].shape[2]), half),
            pltpu.VMEM(routed[0].shape, half),
            pltpu.VMEM(routed[1].shape, half),
            pltpu.VMEM(routed[2].shape, half),
            dma((3,)),
            dma((2, at.deep)),
            dma((at.deep,)),
            dma((at.deep, at.flat)),
            dma((at.deep, at.flat)),
            dma((at.deep, at.flat)),
            dma((at.deep, at.flat)),
            dma((at.deep,)),
            dma((2, at.deep)),
        ],
        compiler_params=pltpu.CompilerParams(
            collective_id=2, has_side_effects=True, vmem_limit_bytes=60 * 1024 * 1024
        ),
    )(normed, middle, select, mix, *common, *routed)


def on_device(
    queries,
    key_matrix,
    value_matrix,
    channel_decay_input,
    head_decay_offset,
    output_gate_input,
    head_norm_gain,
    residual,
    mixer_output_weight,
    expert_norm_gain,
    routes,
    chosen_router_scores,
    routed_gate_weight,
    routed_up_weight,
    routed_down_weight,
    common_gate_weight,
    common_up_weight,
    common_down_weight,
):
    device_heads = head_decay_offset.shape[1]
    seq_rows = queries.shape[0]
    blocks = seq_rows // BLOCK

    def split_local(values, columns):
        return (
            values.astype(jnp.float32)
            .reshape(blocks, BLOCK, device_heads, columns)
            .transpose(2, 0, 1, 3)
        )

    decay_spike_columns = jnp.repeat(head_decay_offset, KEY_CHANNELS, axis=1)
    decay_logarithm = (
        jax.nn.log_sigmoid(channel_decay_input.astype(jnp.float32)) / decay_running
        + decay_spike_columns
    )
    within = jnp.einsum(
        "ij,hnjd->hnid",
        jnp.tril(jnp.ones((BLOCK, BLOCK), jnp.float32)),
        split_local(decay_logarithm, KEY_CHANNELS),
        precision=lax.Precision.HIGHEST,
    )
    block_end = within[:, :, -1, :]
    q_heads = split_local(queries, KEY_CHANNELS) * KEY_CHANNELS ** (-0.5)
    k_heads = split_local(key_matrix, KEY_CHANNELS)
    v_heads = split_local(value_matrix, VDIM)
    q_decay = q_heads * jnp.exp(within)
    k_grow = k_heads * jnp.exp(-within)
    k_tail = k_heads * jnp.exp(block_end[:, :, None, :] - within)
    causal = jnp.tril(jnp.ones((BLOCK, BLOCK), dtype=bool))
    scores = jnp.where(causal, jnp.einsum("hnid,hnjd->hnij", q_decay, k_grow), 0.0)
    inside = jnp.einsum("hnij,hnje->hnie", scores, v_heads)
    block_state = jnp.einsum("hncd,hnce->hnde", k_tail, v_heads)
    inclusive = jnp.cumsum(block_end, axis=1)
    exclusive = inclusive - block_end
    before = jnp.arange(blocks)[:, None] > jnp.arange(blocks)[None, :]
    spread = jnp.exp(
        jnp.where(
            before[None, :, :, None], exclusive[:, :, None, :] - inclusive[:, None, :, :], -jnp.inf
        )
    )
    local_start = jnp.einsum("hnmd,hmde->hnde", spread, block_state)
    total_log = inclusive[:, -1, :]
    tail_weight = jnp.exp(total_log[:, None, :] - inclusive)
    device_state = jnp.einsum("hnd,hnde->hde", tail_weight, block_state)
    lanes = VDIM
    tok_count = residual.shape[0]
    sp_index = lax.axis_index("sp")
    sp_size = lax.axis_size("sp")
    state_rows = device_heads * KEY_CHANNELS
    parts = [
        total_log.reshape(-1, lanes),
        routes.T.astype(jnp.float32).reshape(-1, lanes),
        chosen_router_scores.T.reshape(-1, lanes),
    ]
    stops = [sum(part.shape[0] for part in parts[: i + 1]) for i in range(len(parts))]
    spare = -stops[-1] % 8
    packet = jnp.concatenate(parts + [jnp.zeros((spare, lanes), jnp.float32)], axis=0)
    state = device_state.reshape(state_rows, lanes).astype(jnp.bfloat16)
    states, gathered = gather_sp(state, packet)
    states = states.reshape(sp_size, device_heads, KEY_CHANNELS, VDIM).astype(jnp.float32)
    logs = gathered[:, : stops[0]].reshape(sp_size, device_heads, KEY_CHANNELS)
    ahead = (jnp.arange(sp_size) < sp_index)[:, None, None]
    logs = jnp.where(ahead, logs, 0.0)
    later = (jnp.arange(sp_size)[:, None] < jnp.arange(sp_size)[None, :])[:, :, None, None]
    after = jnp.sum(jnp.where(later, logs[None], 0.0), axis=1)
    reach = jnp.where(ahead, jnp.exp(after), 0.0)
    carried = jnp.sum(reach[..., None] * states, axis=0)
    entering = local_start + jnp.exp(exclusive)[..., None] * carried[:, None, :, :]
    output = inside + jnp.einsum("hncd,hnde->hnce", q_decay, entering)
    output = output.transpose(1, 2, 0, 3).reshape(seq_rows, device_heads, VDIM)
    inv_rms = lax.rsqrt(jnp.mean(output * output, axis=-1, keepdims=True) + eps_norm)
    normed_heads = (output * inv_rms * head_norm_gain).reshape(seq_rows, device_heads * VDIM)
    gated_output = (normed_heads * jax.nn.silu(output_gate_input.astype(jnp.float32))).astype(
        jnp.bfloat16
    )
    stacked = gated_output.reshape(lax.axis_size("tp"), tok_count, gated_output.shape[1])
    projected = jnp.dot(
        swap_tp(stacked), mixer_output_weight, preferred_element_type=jnp.float32
    )
    middle = (residual.astype(jnp.float32) + projected).astype(jnp.bfloat16)
    middle_wide = middle.astype(jnp.float32)
    norm_scale = lax.rsqrt(jnp.mean(middle_wide * middle_wide, axis=-1, keepdims=True) + eps_norm)
    normed = (middle_wide * norm_scale * expert_norm_gain).astype(jnp.bfloat16)
    devices = sp_size * lax.axis_size("tp")
    exp_dev = routed_gate_weight.shape[0]
    cap_slots = 2 * TOP_K * tok_count // (exp_dev * devices)
    at = Place(sp_size, lax.axis_size("tp")).here()
    column = lax.dynamic_index_in_dim(
        gathered.reshape(at.deep, at.rows, -1, lanes), at.b, 1, False
    )
    names = column[:, stops[0] : stops[1]].reshape(at.deep, TOP_K, 1, tok_count)
    scores_all = column[:, stops[1] : stops[2]].reshape(at.deep, TOP_K, 1, tok_count)
    weights = routed_scale * scores_all / jnp.sum(scores_all, axis=1, keepdims=True)
    plane_experts = at.flat * exp_dev
    expert = (at.a * plane_experts + jnp.arange(plane_experts)).astype(jnp.float32)
    hit = (names == expert[None, None, :, None]).astype(jnp.float32)
    chosen = jnp.sum(hit, axis=1)
    weight_of = jnp.sum(hit * weights, axis=1)
    sooner = jnp.triu(jnp.ones((tok_count, tok_count), jnp.bfloat16), 1)
    rank = jnp.einsum(
        "aeu,ut->aet",
        chosen.astype(jnp.bfloat16),
        sooner,
        preferred_element_type=jnp.float32,
    )
    slot = jnp.arange(cap_slots, dtype=jnp.float32)[None, None, :, None]
    taken = (rank[:, :, None, :] == slot) & (chosen[:, :, None, :] > 0.0)
    slots = plane_experts * cap_slots
    select = taken.astype(jnp.bfloat16).reshape(at.deep, slots, tok_count)
    mix = jnp.where(taken, weight_of[:, :, None, :], 0.0).astype(jnp.bfloat16)
    mix = mix.reshape(at.deep, slots, tok_count).transpose(0, 2, 1)
    return experts_layer(
        normed,
        middle,
        select,
        mix,
        (common_gate_weight, common_up_weight, common_down_weight),
        (routed_gate_weight, routed_up_weight, routed_down_weight),
    )


def solution(mesh):
    placed = (
        P("sp", "tp"),
        P("sp", "tp"),
        P("sp", "tp"),
        P("sp", "tp"),
        P("sp", "tp"),
        P("sp", "tp"),
        P(),
        P(("sp", "tp"), None),
        P(),
        P(),
        P(("sp", "tp"), None),
        P(("sp", "tp"), None),
        P(("sp", "tp"), None, None),
        P(("sp", "tp"), None, None),
        P(("sp", "tp"), None, None),
        P(),
        P(),
        P(),
    )
    return jax.shard_map(
        on_device, mesh=mesh, in_specs=placed, out_specs=P(("sp", "tp"), None), check_vma=False
    )
```

time: 338 us -> 184 us (0.54)
  Pallas kernels: 0 us -> 161 us
  blocking collectives: 151 us -> 0 us
  waiting for transfers between devices: 92.8 us -> 0 us
  local copies, waits for them, and re-layouts: 43.2 us -> 9.33 us
  matrix products: 27.7 us -> 5.72 us
  other arithmetic: 14.9 us -> 6.62 us
  starting transfers between devices: 7.35 us -> 0 us
    pallas_call x0 -> x3, Pallas kernels: none -> 161 us  [the longest x1 141 us: experts_layer(): pl.pallas_call(functools.partial(experts_kernel, sizes), out_shape=jax.Sh...]
    all_to_all x1 -> x0, blocking collectives: 96.9 us -> none  [on_device(): lax.all_to_all(outgoing, ('sp', 'tp'), split_axis=0, concat_axis=0, tiled...]
    all_to_all x2 -> x0, waiting for transfers between devices: 92.8 us -> none  [the longest x1 91.5 us: on_device(): lax.all_to_all(produced, ('sp', 'tp'), split_axis=0, concat_axis=0, tiled...]
    all_gather x2 -> x0, blocking collectives: 53.7 us -> none  [carried_in(): gathered = jax.tree.map(lambda a: lax.all_gather(a, axis), part)]
    dot_general x5 -> x3, matrix products: 24.3 us -> 3.95 us  [the longest x1 3.2 us: on_device(): jnp.dot(swap_tp(stacked), mixer_output_weight, preferred_element_type=jnp...]
    gather x2 -> x0, local copies, waits for them, and re-layouts: 14 us -> none  [the longest x1 8 us: on_device(): gathered = flat_back[destination].reshape(tok_count, TOP_K, D)]
    convert_element_type x2 -> x1, local copies, waits for them, and re-layouts: 9.49 us -> 0.86 us  [on_device(): select = taken.astype(jnp.bfloat16).reshape(at.deep, slots, tok_count)]
    all_to_all x2 -> x0, starting transfers between devices: 7.35 us -> none  [the longest x1 3.94 us: on_device(): lax.all_to_all(produced, ('sp', 'tp'), split_axis=0, concat_axis=0, tiled...]
  transfers between devices with their start and end apart: 2 -> 0, of which waited for: 2 -> 0; matrix products, arithmetic and copies ran while one was open for 2% -> 0% of each run, Pallas kernels for 0% -> 0%
where the time goes in v1:
time: 184 us; the launch traced here: 183 us
  Pallas kernels  161 us (88%)
  local copies, waits for them, and re-layouts  9.33 us (5%)
  other arithmetic  6.62 us (4%)
  matrix products  5.72 us (3%)
    pallas_call x1, Pallas kernels, experts_layer(): pl.pallas_call(functools.partial(experts_kernel, sizes), out_shape=jax.Sh...  141 us
    pallas_call x2, Pallas kernels, remote_call(): pl.pallas_call(kernel, out_shape=out_shape, in_specs=[vmem] * len(operand...  20 us

profile of v1, /device:TPU:0, one launch (start us, length us, event | category | flops | bytes accessed | tf_op | source)
XLA Modules:
  0.0 183.4 jit_solution(575246202555431783)
XLA Ops:
  0.0 1.1 copy.60
  1.1 0.9 fusion.34
  2.3 0.6 convolution_bitcast_fusion
  3.0 1.2 reshape.162
  4.2 0.3 reshape.161
  4.6 0.4 fusion.2
  5.5 0.3 fusion.28
  5.9 0.6 convert_element_type.65
  6.7 0.7 maximum_maximum_fusion.y_ref
  7.3 13.3 %shard_map.172 = (bf16[8,128,128]{2,1,0:T(8,128)(2,1)}, f32[8,16,128]{2,1,0:T(8,128)}) custom-call(bf16[128,128]{1,0:T(8,128)(2,1)} %bitcast.95, f32[16,128]{1,0:T(8,128)} %maximum_maximum_fusion.y_ref), custom_call_target="tpu_custom_call" | custom-call | tf_op jit(solution)/shard_map/pallas_call | solution.py:50
  20.6 0.8 slice_reduce_fusion
  21.8 1.2 multiply_reduce_fusion.1
  23.4 0.4 fusion.3
  23.8 0.4 multiply_reduce_fusion
  24.3 0.6 mul.131
  25.0 0.4 copy.72
  25.4 0.9 fusion.24
  26.3 6.7 %shard_map.173 = bf16[128,1024]{1,0:T(8,128)(2,1)} custom-call(bf16[4,128,256]{2,1,0:T(8,128)(2,1)} %bitcast.89), custom_call_target="tpu_custom_call" | custom-call | tf_op jit(solution)/shard_map/pallas_call | solution.py:50
  33.0 3.2 %fusion.4 = (f32[128]{0:T(128)S(1)}, bf16[128,2048]{1,0:T(8,128)(2,1)S(1)}) fusion(bf16[128,1024]{1,0:T(8,128)(2,1)} %shard_map.173, bf16[1024,2048]{1,0:T(8,128)(2,1)} %param.26, bf16[128,2048]{1,0:T(8,128)(2,1)S(1)} %copy-done.2), kind=kOutput, calls=%fused_computation.11 | convolution fusion | flops 538443648 | bytes 5505536 | tf_op jit(solution)/shard_map/dot_general | solution.py:494
  36.2 1.0 fusion.6.x_ref
  38.4 0.9 fusion.31
  39.3 0.9 copy.77.select_ref
  40.2 141.3 %shard_map.174 = bf16[128,2048]{1,0:T(8,128)(2,1)} custom-call(bf16[128,2048]{1,0:T(8,128)(2,1)} %fusion.6.x_ref, bf16[128,2048]{1,0:T(8,128)(2,1)} %copy-done.1, bf16[4,256,128]{2,1,0:T(8,128)(2,1)} %copy.77.select_ref, bf16[4,128,256]{2,1,0:T(8,128)(2,1)} %get-tuple-element.11.mix_ref, bf16[2048,512]{1,0:T(8,128)(2,1)} %gate_ref.1, ...), custom_call_target="tpu_custom_call" | custom-call | tf_op jit(solution)/shard_map/pallas_call | solution.py:363
  181.5 1.9 %copy.127 = bf16[128,2048]{1,0:T(8,128)(2,1)} copy(bf16[128,2048]{1,0:T(8,128)(2,1)} %shard_map.174) | data formatting | bytes 1048576
  (70 shorter events, 3.2 us)
Async XLA Ops:
  0.0 25.4 %copy-start = (f32[128]{0:T(128)S(1)}, f32[128]{0:T(128)}, u32[]{:S(2)}) copy-start(f32[128]{0:T(128)} %param.24) | copy-start | bytes 1540
  0.0 4.2 %copy-start.5 = (bf16[512,128]{1,0:T(8,128)(2,1)S(1)}, bf16[512,128]{1,0:T(8,128)(2,1)}, u32[]{:S(2)}) copy-start(bf16[512,128]{1,0:T(8,128)(2,1)} %param.18) | copy-start | bytes 393220
  0.0 4.6 %copy-start.3 = (bf16[512,256]{1,0:T(8,128)(2,1)S(1)}, bf16[512,256]{1,0:T(8,128)(2,1)}, u32[]{:S(2)}) copy-start(bf16[512,256]{1,0:T(8,128)(2,1)} %param.20) | copy-start | bytes 786436
  2.3 4.2 %copy-start.8 = (s32[128,4]{0,1:T(4,128)S(1)}, s32[128,4]{0,1:T(4,128)}, u32[]{:S(2)}) copy-start(s32[128,4]{0,1:T(4,128)} %param.28) | copy-start | bytes 6148
  2.3 4.3 %copy-start.9 = (f32[128,4]{0,1:T(4,128)S(1)}, f32[128,4]{0,1:T(4,128)}, u32[]{:S(2)}) copy-start(f32[128,4]{0,1:T(4,128)} %param.29) | copy-start | bytes 6148
  5.3 20.1 %copy-start.4 = (bf16[512,256]{1,0:T(8,128)(2,1)S(1)}, bf16[512,256]{1,0:T(8,128)(2,1)}, u32[]{:S(2)}) copy-start(bf16[512,256]{1,0:T(8,128)(2,1)} %param.23) | copy-start | bytes 786436
  23.3 9.6 %copy-start.2 = (bf16[128,2048]{1,0:T(8,128)(2,1)S(1)}, bf16[128,2048]{1,0:T(8,128)(2,1)}, u32[]{:S(2)}) copy-start(bf16[128,2048]{1,0:T(8,128)(2,1)} %param.25) | copy-start | bytes 1572868
  25.0 11.3 %copy-start.7 = (f32[2048]{0:T(1024)S(1)}, f32[2048]{0:T(1024)}, u32[]{:S(2)}) copy-start(f32[2048]{0:T(1024)} %param.27) | copy-start | bytes 24580
  25.4 11.8 %copy-start.6 = (f32[8,16,128]{2,1,0:T(8,128)S(1)}, f32[8,16,128]{2,1,0:T(8,128)}, u32[]{:S(2)}) copy-start(f32[8,16,128]{2,1,0:T(8,128)} %get-tuple-element.7) | copy-start | bytes 196612
  36.2 4.0 %copy-start.1 = (bf16[128,2048]{1,0:T(8,128)(2,1)}, bf16[128,2048]{1,0:T(8,128)(2,1)S(1)}, u32[]{:S(2)}) copy-start(bf16[128,2048]{1,0:T(8,128)(2,1)S(1)} %get-tuple-element.20.middle_ref) | copy-start | bytes 1572868
